TPU v7x, 32 devices: a whole 2x2x4 slice. The times are simulated.
32 devices in a mesh: ep: 8 (over z, y), tp: 4 (over x, core).
Axes of the slice: x: 2, y: 2, z: 4, core: 2. Of those that a mesh axis runs over, the one named last changes fastest.
Arguments:
- tokens: bfloat16 [256, 2048], P('ep'), may hold values from -6 to 6
- kv_cache: bfloat16 [256, 1024, 512], P('ep', None, 'tp'), may hold values from -320 to 320
- lengths: int32 [256], P('ep'), may hold values from 1 to 1024, 131072 in all
- attn_gain: float32 [2048], replicated, may hold values from 0.1 to 1.9
- w_query: bfloat16 [2048, 1024], P(None, 'tp'), may hold values from -0.125 to 0.125
- w_key: bfloat16 [2048, 256], P(None, 'tp'), may hold values from -0.125 to 0.125
- w_value: bfloat16 [2048, 256], P(None, 'tp'), may hold values from -0.125 to 0.125
- lambdas: float32 [16], P('tp'), may hold values from 0.3 to 0.8
- head_gain: float32 [64], replicated, may hold values from 0.1 to 1.9
- w_out: bfloat16 [1024, 2048], replicated, may hold values from -0.1875 to 0.1875
- ffn_gain: float32 [2048], replicated, may hold values from 0.1 to 1.9
- w_shared_gate: bfloat16 [2048, 512], P(None, 'tp'), may hold values from -0.125 to 0.125
- w_shared_up: bfloat16 [2048, 512], P(None, 'tp'), may hold values from -0.125 to 0.125
- w_shared_down: bfloat16 [512, 2048], P('tp'), may hold values from -0.25 to 0.25
- routing: int32 [256, 4], replicated, may hold values from 0 to 31, all different within a row; in each aligned block of 32 rows (0 to 31, 32 to 63, ...) at most 8 rows name the same one
- route_weights: float32 [256, 4], P('ep'), may hold values from 0.1 to 1
- w_exp_gate: bfloat16 [32, 2048, 512], P(('ep', 'tp')), may hold values from -0.125 to 0.125
- w_exp_up: bfloat16 [32, 2048, 512], P(('ep', 'tp')), may hold values from -0.125 to 0.125
- w_exp_down: bfloat16 [32, 512, 2048], P(('ep', 'tp')), may hold values from -0.25 to 0.25
Outputs:
- mixed: bfloat16 [256, 2048], P('ep', 'tp')
Inputs may be any that keep to these rules, and one draw needn't show every extreme that they name: `lengths`: A sequence's cache holds its past keys and values at positions below its length, and the new token follows them; some sequence uses all 1024 positions. `routing`: each row names 4 different experts. Within the rows of one group of 32 sequences (aligned blocks) no expert is named by more than 8 rows, and in some blocks an expert is named by exactly 8.
All inputs are finite; a program needn't handle non-finite values. No bound on the sum of `lengths` on one device may be relied on, other than what follows from the above.
Results may differ from a plain program's by a relative error of at most 0.015.
The roundings to bfloat16 on the way count: a program that leaves them out, or rounds other values in their place, can miss the bound.
Values may be sent and summed in bfloat16 or wider, within the bound.
A program may use at most 128 MiB of HBM per device.

v0:
```python
import functools

import jax
import jax.numpy as jnp
from jax import lax
from jax.experimental import pallas as pl
from jax.experimental.pallas import tpu as pltpu
from jax.sharding import PartitionSpec as P

epsilon = 1e-06
neg_fill = -1e30
MESH = pl.DeviceIdType.MESH
F32 = jnp.float32
BF16 = jnp.bfloat16


def mm(left, right):
    return jnp.dot(left, right, preferred_element_type=F32)


def iota(shape, dim):
    return lax.broadcasted_iota(jnp.int32, shape, dim)


def hot(condition):
    return condition.astype(F32).astype(BF16)


def mm_t(left, right):
    return lax.dot_general(left, right, (((1,), (1,)), ((), ())), preferred_element_type=F32)


def exact(left, right, last):
    return lax.dot_general(
        left,
        right,
        (((1,), (last,)), ((), ())),
        preferred_element_type=F32,
        precision=lax.Precision.HIGHEST,
    )


def rms(values, gain):
    return values * lax.rsqrt(jnp.mean(values * values, axis=-1, keepdims=True) + epsilon) * gain


def flat_slots(values):
    blocks, rows, width = values.shape
    wide = values.astype(F32)
    if rows % 8 == 0:
        return wide.reshape(blocks * rows, width)
    return jnp.concatenate([wide[i] for i in range(blocks)], axis=0)


def layer(
    n_ep,
    n_tp,
    capacity,
    group,
    lengths,
    lambdas,
    tokens,
    attn_gain,
    head_gain,
    ffn_gain,
    routing,
    route_weights,
    kv_hbm,
    wq_hbm,
    wk_hbm,
    wv_hbm,
    wo_hbm,
    sg_hbm,
    su_hbm,
    sd_hbm,
    eg_hbm,
    eu_hbm,
    ed_hbm,
    out,
    kv,
    wq,
    wk,
    wv,
    wo,
    sg,
    su,
    sd,
    eg,
    eu,
    ed,
    q_rows,
    score_new,
    value_new,
    mix_rows,
    heads,
    resid,
    packed,
    arrived,
    computed,
    returned,
    share_out,
    share_in,
    kv_sem,
    w_sem,
    head_send,
    head_recv,
    disp_send,
    disp_recv,
    back_send,
    back_recv,
    share_send,
    share_recv,
):
    n_dev = n_ep * n_tp
    ep = lax.axis_index("ep")
    tp = lax.axis_index("tp")
    me = ep * n_tp + tp
    seqs, width = tokens.shape
    cache_len, lanes = kv.shape[1], kv.shape[2]
    v_width = lanes // 2
    qk_width = v_width // 2
    per_kv = lambdas.shape[0]
    pairs = seqs // 2
    half = 2 * per_kv
    block = 2 * half
    share = width // n_tp
    scaling = qk_width**-0.5
    barrier = pltpu.get_barrier_semaphore()

    weights = [
        pltpu.make_async_copy(src, dst, w_sem.at[i])
        for i, (src, dst) in enumerate(
            [
                (wq_hbm, wq),
                (wk_hbm, wk),
                (wv_hbm, wv),
                (wo_hbm, wo),
                (sg_hbm, sg),
                (su_hbm, su),
                (sd_hbm, sd),
                (eg_hbm.at[0], eg),
                (eu_hbm.at[0], eu),
                (ed_hbm.at[0], ed),
            ]
        )
    ]

    def kv_copy(pair):
        rows = pl.ds(2 * pair, 2)
        return pltpu.make_async_copy(kv_hbm.at[rows], kv.at[rows], kv_sem.at[pair])

    for i in range(3):
        weights[i].start()

    def start_kv(pair, carry):
        kv_copy(pair).start()
        return carry

    lax.fori_loop(0, pairs, start_kv, 0)
    for i in range(3, 10):
        weights[i].start()

    def greet(step, carry):
        other = lax.rem(me + step, n_dev)
        pl.semaphore_signal(
            barrier, inc=1, device_id=(other // n_tp, lax.rem(other, n_tp)), device_id_type=MESH
        )
        return carry

    lax.fori_loop(1, n_dev, greet, 0)

    top_count, batch = routing.shape
    picked = (iota((seqs, batch), 0) + ep * seqs == iota((seqs, batch), 1)).astype(F32)
    own_ids = exact(picked, routing[...].astype(F32), 1).astype(jnp.int32)
    own_weights = exact(
        (iota((seqs, seqs), 0) == iota((seqs, seqs), 1)).astype(F32), route_weights[...], 1
    )
    before = hot(iota((seqs, seqs), 1) < iota((seqs, seqs), 0))

    def slots(count, expert_of):
        column = iota((seqs, count), 1)
        expert = expert_of(column // capacity)
        named = [own_ids[:, k : k + 1] == expert for k in range(top_count)]
        hit = functools.reduce(jnp.logical_or, named)
        rank = mm(before, hot(hit))
        chosen = hit & (rank == lax.rem(column, capacity).astype(F32))
        return named, chosen

    _, chosen = slots(n_ep * capacity, lambda target: target * n_tp + tp)
    dispatch = hot(chosen)
    named_all, chosen_all = slots(n_dev * capacity, lambda expert: expert)
    mixing = jnp.zeros((seqs, n_dev * capacity), F32)
    for k in range(top_count):
        mixing = mixing + jnp.where(named_all[k] & chosen_all, own_weights[:, k : k + 1], 0.0)
    mix_high = mixing.astype(BF16)
    mix_low = (mixing - mix_high.astype(F32)).astype(BF16)

    normed = rms(tokens[...].astype(F32), attn_gain[...]).astype(BF16)
    for i in range(3):
        weights[i].wait()
    queries = mm(normed, wq[...]).astype(BF16)
    key_new = mm_t(normed, wk[...]).astype(BF16)
    val_new = mm_t(normed, wv[...]).astype(BF16)
    spot = (v_width, lanes)
    place_key = hot(iota(spot, 0) == iota(spot, 1))
    place_val = hot(iota(spot, 0) + v_width == iota(spot, 1))
    wide_gain = exact(jnp.broadcast_to(head_gain[...], (8, v_width)), place_val.astype(F32), 0)
    entry_new = (mm(key_new, place_key) + mm(val_new, place_val)).astype(BF16)

    rows = seqs * half
    row = iota((rows, seqs), 0)
    spread = hot(
        row // block * 2 + lax.rem(row, half) // per_kv == iota((rows, seqs), 1)
    )
    wide_q = mm(spread, queries)
    row = iota(wide_q.shape, 0)
    lane = iota(wide_q.shape, 1)
    mine = (lane // v_width == lax.rem(row, per_kv)) & (
        lax.rem(lane, v_width) // qk_width == lax.rem(row, block) // half
    )
    wide_q = jnp.where(mine, wide_q, 0.0).astype(BF16)
    fold = (queries.shape[1], 2 * lanes)
    folded = mm(wide_q, hot(lax.rem(iota(fold, 0), v_width) == lax.rem(iota(fold, 1), lanes)))
    row = iota(folded.shape, 0)
    lane = iota(folded.shape, 1)
    q_rows[...] = jnp.where(lax.rem(row, half) // per_kv == lane // lanes, folded, 0.0).astype(BF16)
    fresh = jnp.sum(folded[:, :lanes] * mm(spread, entry_new), axis=1, keepdims=True) * scaling
    score_new[...] = jnp.broadcast_to(fresh, score_new.shape)
    row = iota((seqs * per_kv, seqs), 0)
    repeat = hot(row // per_kv == iota((seqs * per_kv, seqs), 1))
    value_new[...] = mm(repeat, entry_new)

    row = iota((block, 1), 0)
    factor = jnp.ones((block, 1), F32)
    for g in range(per_kv):
        factor = jnp.where((row >= half) & (lax.rem(row, per_kv) == g), lambdas[g], factor)

    def attend(index, carry):
        first = index * group
        for i in range(group):
            kv_copy(first + i).wait()
        stage = []
        for i in range(group):
            pair = first + i
            both = jnp.concatenate([kv[2 * pair], kv[2 * pair + 1]], axis=1)
            query = q_rows[pl.ds(pl.multiple_of(pair * block, block), block), :]
            stage.append(mm_t(query, both) * scaling)
        weighed = []
        for i in range(group):
            pair = first + i
            fresh = score_new[pl.ds(pl.multiple_of(pair * block, block), block), :][:, :1]
            second = lax.rem(iota((block, 1), 0), half) // per_kv == 1
            limit = jnp.where(second, lengths[2 * pair + 1], lengths[2 * pair])
            valid = iota((block, cache_len), 1) < limit
            scores = jnp.where(valid, stage[i], neg_fill)
            highest = jnp.maximum(jnp.max(scores, axis=1, keepdims=True), fresh)
            expo = jnp.where(valid, jnp.exp(scores - highest), 0.0)
            expo_new = jnp.exp(fresh - highest)
            scale = factor / (jnp.sum(expo, axis=1, keepdims=True) + expo_new)
            expo = expo * scale
            expo_new = expo_new * scale
            weighed.append(
                (
                    (expo[:half] - expo[half:]).astype(BF16),
                    (expo_new[:half] - expo_new[half:]).astype(BF16).astype(F32),
                )
            )
        for i in range(group):
            pair = first + i
            both = jnp.concatenate([kv[2 * pair], kv[2 * pair + 1]], axis=1)
            mixed = mm(weighed[i][0], both)
            upper = iota((half, lanes), 0) < per_kv
            mixed = jnp.where(upper, mixed[:, :lanes], mixed[:, lanes:])
            spots = pl.ds(pl.multiple_of(pair * half, half), half)
            mix_rows[spots, :] = mixed + weighed[i][1] * value_new[spots, :]
        return carry

    lax.fori_loop(0, pairs // group, attend, 0)

    mixed = mix_rows[...]
    squares = jnp.where(iota(mixed.shape, 1) >= v_width, mixed * mixed, 0.0)
    mean = jnp.sum(squares, axis=1, keepdims=True) * (1.0 / v_width)
    head_out = (mixed * lax.rsqrt(mean + epsilon) * wide_gain[:1]).astype(BF16)
    unfold = (lanes, per_kv * v_width)
    shifted = hot(lax.rem(iota(unfold, 1), v_width) + v_width == iota(unfold, 0))
    laid = mm(head_out, shifted)
    own = iota(laid.shape, 1) // v_width == lax.rem(iota(laid.shape, 0), per_kv)
    laid = jnp.where(own, laid, 0.0).astype(BF16)
    gather = (seqs, seqs * per_kv)
    heads[tp] = mm(hot(iota(gather, 1) // per_kv == iota(gather, 0)), laid).astype(BF16)

    pl.semaphore_wait(barrier, n_dev - 1)

    def head_copy(step):
        other = lax.rem(tp + step, n_tp)
        return pltpu.make_async_remote_copy(
            src_ref=heads.at[tp],
            dst_ref=heads.at[tp],
            send_sem=head_send.at[step],
            recv_sem=head_recv.at[step],
            device_id=(ep, other),
            device_id_type=MESH,
        )

    head_copies = [head_copy(step) for step in range(1, n_tp)]
    for copy in head_copies:
        copy.start()
    weights[3].wait()
    for copy in head_copies:
        copy.wait_recv()
    depth = heads.shape[2]
    projected = jnp.zeros((seqs, width), F32)
    for i in range(n_tp):
        piece = mm(heads[i], wo[i * depth : (i + 1) * depth, :])
        projected = projected + piece.astype(BF16).astype(F32)
    residual = (tokens[...].astype(F32) + projected).astype(BF16).astype(F32)
    for i in range(n_tp):
        resid[i] = residual[:, i * share : (i + 1) * share]
    ffn_in = rms(residual, ffn_gain[...]).astype(BF16)

    sorted_rows = lax.dot_general(
        dispatch, ffn_in, (((0,), (0,)), ((), ())), preferred_element_type=F32
    )
    for e in range(n_ep):
        packed[e] = sorted_rows[e * capacity : (e + 1) * capacity, :].astype(BF16)
    arrived[ep] = packed[ep]

    def disp_copy(step):
        other = lax.rem(ep + step, n_ep)
        return pltpu.make_async_remote_copy(
            src_ref=packed.at[other],
            dst_ref=arrived.at[ep],
            send_sem=disp_send.at[step],
            recv_sem=disp_recv.at[step],
            device_id=(other, tp),
            device_id_type=MESH,
        )

    def loop(make, act, count):
        def body(step, carry):
            act(make(step))
            return carry

        lax.fori_loop(1, count, body, 0)

    loop(disp_copy, lambda copy: copy.start(), n_ep)

    for i in range(4, 7):
        weights[i].wait()
    shared_act = (jax.nn.silu(mm(ffn_in, sg[...])) * mm(ffn_in, su[...])).astype(BF16)
    shared_part = mm(shared_act, sd[...])
    for i in range(n_tp):
        share_out[i] = shared_part[:, i * share : (i + 1) * share].astype(BF16)

    def share_copy(step):
        other = lax.rem(tp + step, n_tp)
        return pltpu.make_async_remote_copy(
            src_ref=share_out.at[other],
            dst_ref=share_in.at[step],
            send_sem=share_send.at[step],
            recv_sem=share_recv.at[step],
            device_id=(ep, other),
            device_id_type=MESH,
        )

    share_copies = [share_copy(step) for step in range(1, n_tp)]
    for copy in share_copies:
        copy.start()

    for i in range(7, 10):
        weights[i].wait()
    loop(disp_copy, lambda copy: copy.wait_recv(), n_ep)
    flat = flat_slots(arrived[...]).astype(BF16)
    act = (jax.nn.silu(mm(flat, eg[...])) * mm(flat, eu[...])).astype(BF16)
    result = mm(act, ed[...])
    for e in range(n_ep):
        for t in range(n_tp):
            computed[e * n_tp + t] = result[
                e * capacity : (e + 1) * capacity, t * share : (t + 1) * share
            ].astype(BF16)
    returned[me] = computed[me]

    def back_copy(step):
        other = lax.rem(me + step, n_dev)
        return pltpu.make_async_remote_copy(
            src_ref=computed.at[other],
            dst_ref=returned.at[me],
            send_sem=back_send.at[step],
            recv_sem=back_recv.at[step],
            device_id=(other // n_tp, lax.rem(other, n_tp)),
            device_id_type=MESH,
        )

    loop(back_copy, lambda copy: copy.start(), n_dev)
    total = resid[tp] + share_out[tp].astype(F32)
    for step, copy in enumerate(share_copies):
        copy.wait_recv()
        total = total + share_in[step + 1].astype(F32)
    loop(back_copy, lambda copy: copy.wait_recv(), n_dev)
    back = flat_slots(returned[...]).astype(BF16)
    routed = mm(mix_high, back) + mm(mix_low, back)
    out[...] = (total + routed).astype(BF16)

    for copy in head_copies + share_copies:
        copy.wait_send()
    loop(disp_copy, lambda copy: copy.wait_send(), n_ep)
    loop(back_copy, lambda copy: copy.wait_send(), n_dev)


def shards(
    n_ep,
    n_tp,
    tokens,
    kv_cache,
    lengths,
    attn_gain,
    w_query,
    w_key,
    w_value,
    lambdas,
    head_gain,
    w_out,
    ffn_gain,
    w_shared_gate,
    w_shared_up,
    w_shared_down,
    routing,
    route_weights,
    w_exp_gate,
    w_exp_up,
    w_exp_down,
):
    seqs, width = tokens.shape
    lanes = kv_cache.shape[2]
    v_width = head_gain.shape[0]
    per_kv = lambdas.shape[0]
    n_dev = n_ep * n_tp
    capacity = max(2, 2 * seqs * routing.shape[1] // (w_exp_gate.shape[0] * n_dev))
    share = width // n_tp
    half = 2 * per_kv
    pairs = seqs // 2
    group = next(g for g in (8, 4, 2, 1) if pairs % g == 0)
    big = [
        kv_cache,
        w_query,
        w_key.T,
        w_value.T,
        w_out,
        w_shared_gate,
        w_shared_up,
        w_shared_down,
        w_exp_gate,
        w_exp_up,
        w_exp_down,
    ]
    held = [pltpu.VMEM(x.shape, BF16) for x in big[:8]]
    held += [pltpu.VMEM(x.shape[1:], BF16) for x in big[8:]]
    vmem = pl.BlockSpec(memory_space=pltpu.VMEM)
    smem = pl.BlockSpec(memory_space=pltpu.SMEM)
    dma = pltpu.SemaphoreType.DMA
    return pl.pallas_call(
        functools.partial(layer, n_ep, n_tp, capacity, group),
        out_shape=jax.ShapeDtypeStruct((seqs, share), BF16),
        in_specs=[smem] * 2 + [vmem] * 6 + [pl.BlockSpec(memory_space=pltpu.HBM)] * len(big),
        out_specs=vmem,
        scratch_shapes=held
        + [
            pltpu.VMEM((seqs * half, 2 * lanes), BF16),
            pltpu.VMEM((seqs * half, lanes), F32),
            pltpu.VMEM((seqs * per_kv, lanes), F32),
            pltpu.VMEM((seqs * per_kv, lanes), F32),
            pltpu.VMEM((n_tp, seqs, per_kv * v_width), BF16),
            pltpu.VMEM((n_tp, seqs, share), F32),
            pltpu.VMEM((n_ep, capacity, width), BF16),
            pltpu.VMEM((n_ep, capacity, width), BF16),
            pltpu.VMEM((n_dev, capacity, share), BF16),
            pltpu.VMEM((n_dev, capacity, share), BF16),
            pltpu.VMEM((n_tp, seqs, share), BF16),
            pltpu.VMEM((n_tp, seqs, share), BF16),
            dma((pairs,)),
            dma((10,)),
            dma((n_tp,)),
            dma((n_tp,)),
            dma((n_ep,)),
            dma((n_ep,)),
            dma((n_dev,)),
            dma((n_dev,)),
            dma((n_tp,)),
            dma((n_tp,)),
        ],
        compiler_params=pltpu.CompilerParams(
            collective_id=0, has_side_effects=True, vmem_limit_bytes=60 * 1024 * 1024
        ),
    )(
        lengths,
        lambdas,
        tokens,
        attn_gain[None, :],
        head_gain[None, :],
        ffn_gain[None, :],
        routing.T,
        route_weights.T,
        *big,
    )


def solution(mesh):
    return jax.shard_map(
        functools.partial(shards, mesh.shape["ep"], mesh.shape["tp"]),
        mesh=mesh,
        in_specs=(
            P("ep", None),
            P("ep", None, "tp"),
            P("ep"),
            P(),
            P(None, "tp"),
            P(None, "tp"),
            P(None, "tp"),
            P("tp"),
            P(),
            P(),
            P(),
            P(None, "tp"),
            P(None, "tp"),
            P("tp", None),
            P(),
            P("ep", None),
            P(("ep", "tp"), None, None),
            P(("ep", "tp"), None, None),
            P(("ep", "tp"), None, None),
        ),
        out_specs=P("ep", "tp"),
        check_vma=False,
    )
```

profile of v0, /device:TPU:0, one launch (start us, length us, event | category | flops | bytes accessed | tf_op | source)
XLA Modules:
  0.0 32.4 jit_solution(8872636106253306981)
XLA Ops:
  0.0 31.0 %shard_map.181 = bf16[32,512]{1,0:T(8,128)(2,1)} custom-call(s32[32]{0:T(128)} %lengths.1, f32[4]{0:T(128)} %lambdas.1, bf16[32,2048]{1,0:T(8,128)(2,1)} %tokens.1, f32[1,2048]{1,0:T(1,128)} %bitcast.9, f32[1,64]{1,0:T(1,128)} %bitcast.13, f32[1,2048]{1,0:T(1,128)} %bitcast.10, s32[4,256]{1,0:T(4,128)} %bitcast.11, f32[4,32]{1,0:T(4,128)} %bitcast.12, ...), custom_call_target="tpu_custom_call" | custom-call | tf_op jit(solution)/shard_map/pallas_call | solution.py:461
  31.0 1.4 %copy.21 = bf16[32,512]{1,0:T(8,128)(2,1)} copy(bf16[32,512]{1,0:T(8,128)(2,1)} %shard_map.181) | data formatting | bytes 65536
where the time goes:
time: 32.5 us; the launch traced here: 32.4 us
  Pallas kernels  31 us (95%)
  local copies, waits for them, and re-layouts  1.38 us (4%)
    pallas_call x1, Pallas kernels, shards(): pl.pallas_call(functools.partial(layer, n_ep, n_tp, capacity, group), out...  31 us
    unnamed x1, local copies, waits for them, and re-layouts  1.38 us

commit v1 on v0

--- a/solution.py
+++ b/solution.py
@@ -57,14 +57,14 @@
     n_tp,
     capacity,
     group,
-    lengths,
-    lambdas,
-    tokens,
-    attn_gain,
-    head_gain,
-    ffn_gain,
-    routing,
-    route_weights,
+    lengths_hbm,
+    lambdas_hbm,
+    tokens_hbm,
+    attn_gain_hbm,
+    head_gain_hbm,
+    ffn_gain_hbm,
+    routing_hbm,
+    route_weights_hbm,
     kv_hbm,
     wq_hbm,
     wk_hbm,
@@ -77,6 +77,14 @@
     eu_hbm,
     ed_hbm,
     out,
+    lengths,
+    lambdas,
+    tokens,
+    attn_gain,
+    head_gain,
+    ffn_gain,
+    routing,
+    route_weights,
     kv,
     wq,
     wk,
@@ -100,6 +108,7 @@
     returned,
     share_out,
     share_in,
+    in_sem,
     kv_sem,
     w_sem,
     head_send,
@@ -120,13 +129,29 @@
     v_width = lanes // 2
     qk_width = v_width // 2
     per_kv = lambdas.shape[0]
-    pairs = seqs // 2
-    half = 2 * per_kv
+    side = lanes // v_width * 2
+    packs = seqs // side
+    half = side * per_kv
     block = 2 * half
     share = width // n_tp
     scaling = qk_width**-0.5
     barrier = pltpu.get_barrier_semaphore()
 
+    inputs = [
+        pltpu.make_async_copy(source, target, in_sem.at[i])
+        for i, (source, target) in enumerate(
+            [
+                (tokens_hbm, tokens),
+                (attn_gain_hbm, attn_gain),
+                (routing_hbm, routing),
+                (route_weights_hbm, route_weights),
+                (head_gain_hbm, head_gain),
+                (lambdas_hbm, lambdas),
+                (lengths_hbm, lengths),
+                (ffn_gain_hbm, ffn_gain),
+            ]
+        )
+    ]
     weights = [
         pltpu.make_async_copy(src, dst, w_sem.at[i])
         for i, (src, dst) in enumerate(
@@ -145,20 +170,16 @@
         )
     ]
 
-    def kv_copy(pair):
-        rows = pl.ds(2 * pair, 2)
-        return pltpu.make_async_copy(kv_hbm.at[rows], kv.at[rows], kv_sem.at[pair])
-
+    def kv_copy(pack):
+        rows = pl.ds(side * pack, side)
+        return pltpu.make_async_copy(kv_hbm.at[rows], kv.at[rows], kv_sem.at[pack])
+
+    inputs[0].start()
+    inputs[1].start()
     for i in range(3):
         weights[i].start()
-
-    def start_kv(pair, carry):
-        kv_copy(pair).start()
-        return carry
-
-    lax.fori_loop(0, pairs, start_kv, 0)
-    for i in range(3, 10):
-        weights[i].start()
+    for i in range(2, 8):
+        inputs[i].start()
 
     def greet(step, carry):
         other = lax.rem(me + step, n_dev)
@@ -169,8 +190,19 @@
 
     lax.fori_loop(1, n_dev, greet, 0)
 
+    def start_kv(pack, carry):
+        kv_copy(pack).start()
+        return carry
+
+    lax.fori_loop(0, packs, start_kv, 0)
+
+    for i in range(2):
+        inputs[i].wait()
+    normed = rms(tokens[...].astype(F32), attn_gain[...]).astype(BF16)
     top_count, batch = routing.shape
     picked = (iota((seqs, batch), 0) + ep * seqs == iota((seqs, batch), 1)).astype(F32)
+    for i in range(2, 4):
+        inputs[i].wait()
     own_ids = exact(picked, routing[...].astype(F32), 1).astype(jnp.int32)
     own_weights = exact(
         (iota((seqs, seqs), 0) == iota((seqs, seqs), 1)).astype(F32), route_weights[...], 1
@@ -195,23 +227,18 @@
     mix_high = mixing.astype(BF16)
     mix_low = (mixing - mix_high.astype(F32)).astype(BF16)
 
-    normed = rms(tokens[...].astype(F32), attn_gain[...]).astype(BF16)
     for i in range(3):
         weights[i].wait()
     queries = mm(normed, wq[...]).astype(BF16)
     key_new = mm_t(normed, wk[...]).astype(BF16)
     val_new = mm_t(normed, wv[...]).astype(BF16)
-    spot = (v_width, lanes)
-    place_key = hot(iota(spot, 0) == iota(spot, 1))
-    place_val = hot(iota(spot, 0) + v_width == iota(spot, 1))
-    wide_gain = exact(jnp.broadcast_to(head_gain[...], (8, v_width)), place_val.astype(F32), 0)
-    entry_new = (mm(key_new, place_key) + mm(val_new, place_val)).astype(BF16)
-
-    rows = seqs * half
+    fold_width = side * v_width
+    spot = (v_width, fold_width)
+    tile = hot(iota(spot, 0) == lax.rem(iota(spot, 1), v_width))
+
+    rows = seqs * 2 * per_kv
     row = iota((rows, seqs), 0)
-    spread = hot(
-        row // block * 2 + lax.rem(row, half) // per_kv == iota((rows, seqs), 1)
-    )
+    spread = hot(row // block * side + lax.rem(row, half) // per_kv == iota((rows, seqs), 1))
     wide_q = mm(spread, queries)
     row = iota(wide_q.shape, 0)
     lane = iota(wide_q.shape, 1)
@@ -219,43 +246,62 @@
         lax.rem(lane, v_width) // qk_width == lax.rem(row, block) // half
     )
     wide_q = jnp.where(mine, wide_q, 0.0).astype(BF16)
-    fold = (queries.shape[1], 2 * lanes)
-    folded = mm(wide_q, hot(lax.rem(iota(fold, 0), v_width) == lax.rem(iota(fold, 1), lanes)))
+    fold = (queries.shape[1], fold_width)
+    folded = mm(wide_q, hot(lax.rem(iota(fold, 0), v_width) == lax.rem(iota(fold, 1), v_width)))
     row = iota(folded.shape, 0)
     lane = iota(folded.shape, 1)
-    q_rows[...] = jnp.where(lax.rem(row, half) // per_kv == lane // lanes, folded, 0.0).astype(BF16)
-    fresh = jnp.sum(folded[:, :lanes] * mm(spread, entry_new), axis=1, keepdims=True) * scaling
+    folded = jnp.where(lax.rem(row, half) // per_kv == lane // v_width, folded, 0.0)
+    q_rows[...] = folded.astype(BF16)
+    keys_wide = mm(spread, mm(key_new, tile).astype(BF16))
+    fresh = jnp.sum(folded * keys_wide, axis=1, keepdims=True)
     score_new[...] = jnp.broadcast_to(fresh, score_new.shape)
     row = iota((seqs * per_kv, seqs), 0)
     repeat = hot(row // per_kv == iota((seqs * per_kv, seqs), 1))
-    value_new[...] = mm(repeat, entry_new)
-
+    value_new[...] = mm(repeat, mm(val_new, tile).astype(BF16))
+
+    for i in range(4, 8):
+        inputs[i].wait()
+    wide_gain = exact(jnp.broadcast_to(head_gain[...], (8, v_width)), tile.astype(F32), 0)
     row = iota((block, 1), 0)
     factor = jnp.ones((block, 1), F32)
     for g in range(per_kv):
         factor = jnp.where((row >= half) & (lax.rem(row, per_kv) == g), lambdas[g], factor)
+
+    for i in range(3, 10):
+        weights[i].start()
 
     def attend(index, carry):
         first = index * group
         for i in range(group):
             kv_copy(first + i).wait()
         stage = []
+        values = []
         for i in range(group):
-            pair = first + i
-            both = jnp.concatenate([kv[2 * pair], kv[2 * pair + 1]], axis=1)
-            query = q_rows[pl.ds(pl.multiple_of(pair * block, block), block), :]
-            stage.append(mm_t(query, both) * scaling)
+            pack = first + i
+            keys = []
+            swapped = []
+            for j in range(0, side, 2):
+                even = kv[side * pack + j]
+                odd = pltpu.roll(kv[side * pack + j + 1], v_width, 1)
+                keys += [even[:, :v_width], odd[:, v_width:]]
+                swapped += [odd[:, :v_width], even[:, v_width:]]
+            keys = jnp.concatenate(keys, axis=1)
+            values.append(jnp.concatenate(swapped, axis=1))
+            query = q_rows[pl.ds(pl.multiple_of(pack * block, block), block), :]
+            stage.append(mm_t(query, keys))
         weighed = []
         for i in range(group):
-            pair = first + i
-            fresh = score_new[pl.ds(pl.multiple_of(pair * block, block), block), :][:, :1]
-            second = lax.rem(iota((block, 1), 0), half) // per_kv == 1
-            limit = jnp.where(second, lengths[2 * pair + 1], lengths[2 * pair])
+            pack = first + i
+            fresh = score_new[pl.ds(pl.multiple_of(pack * block, block), block), :][:, :1]
+            owner = lax.rem(iota((block, 1), 0), half) // per_kv
+            limit = jnp.zeros((block, 1), jnp.int32)
+            for j in range(side):
+                limit = jnp.where(owner == j, lengths[side * pack + j], limit)
             valid = iota((block, cache_len), 1) < limit
             scores = jnp.where(valid, stage[i], neg_fill)
             highest = jnp.maximum(jnp.max(scores, axis=1, keepdims=True), fresh)
-            expo = jnp.where(valid, jnp.exp(scores - highest), 0.0)
-            expo_new = jnp.exp(fresh - highest)
+            expo = jnp.exp((scores - highest) * scaling)
+            expo_new = jnp.exp((fresh - highest) * scaling)
             scale = factor / (jnp.sum(expo, axis=1, keepdims=True) + expo_new)
             expo = expo * scale
             expo_new = expo_new * scale
@@ -266,23 +312,21 @@
                 )
             )
         for i in range(group):
-            pair = first + i
-            both = jnp.concatenate([kv[2 * pair], kv[2 * pair + 1]], axis=1)
-            mixed = mm(weighed[i][0], both)
-            upper = iota((half, lanes), 0) < per_kv
-            mixed = jnp.where(upper, mixed[:, :lanes], mixed[:, lanes:])
-            spots = pl.ds(pl.multiple_of(pair * half, half), half)
-            mix_rows[spots, :] = mixed + weighed[i][1] * value_new[spots, :]
+            pack = first + i
+            spots = pl.ds(pl.multiple_of(pack * half, half), half)
+            mixed = mm(weighed[i][0], values[i]) + weighed[i][1] * value_new[spots, :]
+            owner = iota(mixed.shape, 0) // per_kv
+            own = owner + 1 - 2 * lax.rem(owner, 2) == iota(mixed.shape, 1) // v_width
+            mix_rows[spots, :] = jnp.where(own, mixed, 0.0)
         return carry
 
-    lax.fori_loop(0, pairs // group, attend, 0)
+    lax.fori_loop(0, packs // group, attend, 0)
 
     mixed = mix_rows[...]
-    squares = jnp.where(iota(mixed.shape, 1) >= v_width, mixed * mixed, 0.0)
-    mean = jnp.sum(squares, axis=1, keepdims=True) * (1.0 / v_width)
+    mean = jnp.sum(mixed * mixed, axis=1, keepdims=True) * (1.0 / v_width)
     head_out = (mixed * lax.rsqrt(mean + epsilon) * wide_gain[:1]).astype(BF16)
-    unfold = (lanes, per_kv * v_width)
-    shifted = hot(lax.rem(iota(unfold, 1), v_width) + v_width == iota(unfold, 0))
+    unfold = (fold_width, per_kv * v_width)
+    shifted = hot(lax.rem(iota(unfold, 1), v_width) == lax.rem(iota(unfold, 0), v_width))
     laid = mm(head_out, shifted)
     own = iota(laid.shape, 1) // v_width == lax.rem(iota(laid.shape, 0), per_kv)
     laid = jnp.where(own, laid, 0.0).astype(BF16)
@@ -437,9 +481,21 @@
     n_dev = n_ep * n_tp
     capacity = max(2, 2 * seqs * routing.shape[1] // (w_exp_gate.shape[0] * n_dev))
     share = width // n_tp
-    half = 2 * per_kv
-    pairs = seqs // 2
-    group = next(g for g in (8, 4, 2, 1) if pairs % g == 0)
+    side = lanes // v_width * 2
+    packs = seqs // side
+    rows = seqs * per_kv
+    fold = side * v_width
+    group = next(g for g in (4, 2, 1) if packs % g == 0)
+    small = [
+        lengths,
+        lambdas,
+        tokens,
+        attn_gain[None, :],
+        head_gain[None, :],
+        ffn_gain[None, :],
+        routing.T,
+        route_weights.T,
+    ]
     big = [
         kv_cache,
         w_query,
@@ -453,22 +509,23 @@
         w_exp_up,
         w_exp_down,
     ]
-    held = [pltpu.VMEM(x.shape, BF16) for x in big[:8]]
+    held = [pltpu.SMEM(x.shape, x.dtype) for x in small[:2]]
+    held += [pltpu.VMEM(x.shape, x.dtype) for x in small[2:]]
+    held += [pltpu.VMEM(x.shape, BF16) for x in big[:8]]
     held += [pltpu.VMEM(x.shape[1:], BF16) for x in big[8:]]
     vmem = pl.BlockSpec(memory_space=pltpu.VMEM)
-    smem = pl.BlockSpec(memory_space=pltpu.SMEM)
     dma = pltpu.SemaphoreType.DMA
     return pl.pallas_call(
         functools.partial(layer, n_ep, n_tp, capacity, group),
-        out_shape=jax.ShapeDtypeStruct((seqs, share), BF16),
-        in_specs=[smem] * 2 + [vmem] * 6 + [pl.BlockSpec(memory_space=pltpu.HBM)] * len(big),
+        out_shape=pltpu.VMEM((seqs, share), BF16),
+        in_specs=[pl.BlockSpec(memory_space=pltpu.HBM)] * (len(small) + len(big)),
         out_specs=vmem,
         scratch_shapes=held
         + [
-            pltpu.VMEM((seqs * half, 2 * lanes), BF16),
-            pltpu.VMEM((seqs * half, lanes), F32),
-            pltpu.VMEM((seqs * per_kv, lanes), F32),
-            pltpu.VMEM((seqs * per_kv, lanes), F32),
+            pltpu.VMEM((2 * rows, fold), BF16),
+            pltpu.VMEM((2 * rows, lanes), F32),
+            pltpu.VMEM((rows, fold), F32),
+            pltpu.VMEM((rows, fold), F32),
             pltpu.VMEM((n_tp, seqs, per_kv * v_width), BF16),
             pltpu.VMEM((n_tp, seqs, share), F32),
             pltpu.VMEM((n_ep, capacity, width), BF16),
@@ -477,7 +534,8 @@
             pltpu.VMEM((n_dev, capacity, share), BF16),
             pltpu.VMEM((n_tp, seqs, share), BF16),
             pltpu.VMEM((n_tp, seqs, share), BF16),
-            dma((pairs,)),
+            dma((len(small),)),
+            dma((packs,)),
             dma((10,)),
             dma((n_tp,)),
             dma((n_tp,)),
@@ -492,14 +550,7 @@
             collective_id=0, has_side_effects=True, vmem_limit_bytes=60 * 1024 * 1024
         ),
     )(
-        lengths,
-        lambdas,
-        tokens,
-        attn_gain[None, :],
-        head_gain[None, :],
-        ffn_gain[None, :],
-        routing.T,
-        route_weights.T,
+        *small,
         *big,
     )
 

time: 32.5 us -> 30 us (0.923)
  Pallas kernels: 31 us -> 29.3 us
  local copies, waits for them, and re-layouts: 1.38 us -> 0.62 us
    pallas_call x1, Pallas kernels: 31 us -> 29.3 us  [shards(): pl.pallas_call(functools.partial(layer, n_ep, n_tp, capacity, group), out...]
    unnamed x1, local copies, waits for them, and re-layouts: 1.38 us -> 0.62 us
where the time goes in v1:
time: 30 us; the launch traced here: 29.9 us
  Pallas kernels  29.3 us (98%)
  local copies, waits for them, and re-layouts  0.62 us (2%)
    pallas_call x1, Pallas kernels, shards(): pl.pallas_call(functools.partial(layer, n_ep, n_tp, capacity, group), out...  29.3 us
    unnamed x1, local copies, waits for them, and re-layouts  0.62 us

profile of v1, /device:TPU:0, one launch (start us, length us, event | category | flops | bytes accessed | tf_op | source)
XLA Modules:
  0.0 29.9 jit_solution(8369979708931796660)
XLA Ops:
  0.0 29.3 %shard_map.181 = bf16[32,512]{1,0:T(8,128)(2,1)S(1)} custom-call(s32[32]{0:T(128)} %lengths_hbm.1, f32[4]{0:T(128)} %lambdas_hbm.1, bf16[32,2048]{1,0:T(8,128)(2,1)} %tokens_hbm.1, f32[1,2048]{1,0:T(1,128)} %bitcast.9, f32[1,64]{1,0:T(1,128)} %bitcast.13, f32[1,2048]{1,0:T(1,128)} %bitcast.10, s32[4,256]{1,0:T(4,128)} %bitcast.11, f32[4,32]{1,0:T(4,128)} %bitcast.12, ...), custom_call_target="tpu_custom_call" | custom-call | tf_op jit(solution)/shard_map/pallas_call | solution.py:518
  29.3 0.6 %copy.21 = bf16[32,512]{1,0:T(8,128)(2,1)} copy(bf16[32,512]{1,0:T(8,128)(2,1)S(1)} %shard_map.181) | data formatting | bytes 65536

commit v2 on v1

--- a/solution.py
+++ b/solution.py
@@ -101,7 +101,11 @@
     value_new,
     mix_rows,
     heads,
+    head_rows,
+    head_slots,
     resid,
+    relay_pick,
+    relay,
     packed,
     arrived,
     computed,
@@ -111,19 +115,22 @@
     in_sem,
     kv_sem,
     w_sem,
-    head_send,
-    head_recv,
-    disp_send,
-    disp_recv,
-    back_send,
-    back_recv,
-    share_send,
-    share_recv,
+    head_sem,
+    slot_sem,
+    relay_sem,
+    disp_sem,
+    back_sem,
+    share_sem,
 ):
     n_dev = n_ep * n_tp
     ep = lax.axis_index("ep")
     tp = lax.axis_index("tp")
     me = ep * n_tp + tp
+    n_hi, plane = packed.shape[:2]
+    n_lo = n_ep // n_hi
+    hi = ep // n_lo
+    lo = lax.rem(ep, n_lo)
+    spot_in_plane = lo * n_tp + tp
     seqs, width = tokens.shape
     cache_len, lanes = kv.shape[1], kv.shape[2]
     v_width = lanes // 2
@@ -196,6 +203,47 @@
 
     lax.fori_loop(0, packs, start_kv, 0)
 
+    def remote(source, target, sem, other_ep, other_tp):
+        return pltpu.make_async_remote_copy(
+            src_ref=source,
+            dst_ref=target,
+            send_sem=sem.at[0],
+            recv_sem=sem.at[1],
+            device_id=(other_ep, other_tp),
+            device_id_type=MESH,
+        )
+
+    def whole(source, target, sem, count):
+        part = pl.ds(0, count)
+        return remote(
+            source.at[part], target.at[part], sem, lax.rem(ep + 1, n_ep), lax.rem(tp + 1, n_tp)
+        )
+
+    def far_first(step, mine, count):
+        late = 2 * mine // count
+        up = count - 1 - step
+        up = up - (mine >= up).astype(jnp.int32)
+        down = step + (step >= mine).astype(jnp.int32)
+        return (1 - late) * up + late * down
+
+    peers = [
+        (far_first(k, ep, n_ep), lax.rem(tp + t, n_tp))
+        for k in range(n_ep - 1)
+        for t in range(n_tp)
+    ]
+    peers += [(ep, lax.rem(tp + t, n_tp)) for t in range(1, n_tp)]
+    far_planes = [far_first(k, hi, n_hi) for k in range(n_hi - 1)]
+
+    def relay_copy(source, target):
+        return pltpu.make_async_remote_copy(
+            src_ref=tokens.at[:, pl.ds(pl.multiple_of(tp * share, share), share)],
+            dst_ref=relay.at[source],
+            send_sem=relay_sem.at[0],
+            recv_sem=relay_sem.at[1 + source],
+            device_id=(target * n_lo + lo, tp),
+            device_id_type=MESH,
+        )
+
     for i in range(2):
         inputs[i].wait()
     normed = rms(tokens[...].astype(F32), attn_gain[...]).astype(BF16)
@@ -218,12 +266,28 @@
         chosen = hit & (rank == lax.rem(column, capacity).astype(F32))
         return named, chosen
 
-    _, chosen = slots(n_ep * capacity, lambda target: target * n_tp + tp)
-    dispatch = hot(chosen)
     named_all, chosen_all = slots(n_dev * capacity, lambda expert: expert)
     mixing = jnp.zeros((seqs, n_dev * capacity), F32)
     for k in range(top_count):
         mixing = mixing + jnp.where(named_all[k] & chosen_all, own_weights[:, k : k + 1], 0.0)
+    row = iota((seqs * per_kv, seqs), 0)
+    repeat = hot(row // per_kv == iota((seqs * per_kv, seqs), 1))
+    row_choice = mm(repeat, hot(chosen_all)).astype(BF16)
+    relayed = n_hi * seqs
+    row = iota((relayed, batch), 0)
+    picked = (row // seqs * n_lo + lo) * seqs + lax.rem(row, seqs) == iota((relayed, batch), 1)
+    relay_ids = exact(picked.astype(F32), routing[...].astype(F32), 1).astype(jnp.int32)
+    column = iota((relayed, plane * capacity), 1)
+    expert = hi * plane + column // capacity
+    hit = functools.reduce(
+        jnp.logical_or, [relay_ids[:, k : k + 1] == expert for k in range(top_count)]
+    )
+    row, other = iota((relayed, relayed), 0), iota((relayed, relayed), 1)
+    earlier = hot((row // seqs == other // seqs) & (other < row))
+    chosen = hit & (mm(earlier, hot(hit)) == lax.rem(column, capacity).astype(F32))
+    chosen = hot(chosen)
+    for i in range(n_hi):
+        relay_pick[i] = chosen[i * seqs : (i + 1) * seqs, :]
     mix_high = mixing.astype(BF16)
     mix_low = (mixing - mix_high.astype(F32)).astype(BF16)
 
@@ -255,8 +319,6 @@
     keys_wide = mm(spread, mm(key_new, tile).astype(BF16))
     fresh = jnp.sum(folded * keys_wide, axis=1, keepdims=True)
     score_new[...] = jnp.broadcast_to(fresh, score_new.shape)
-    row = iota((seqs * per_kv, seqs), 0)
-    repeat = hot(row // per_kv == iota((seqs * per_kv, seqs), 1))
     value_new[...] = mm(repeat, mm(val_new, tile).astype(BF16))
 
     for i in range(4, 8):
@@ -320,7 +382,16 @@
             mix_rows[spots, :] = jnp.where(own, mixed, 0.0)
         return carry
 
-    lax.fori_loop(0, packs // group, attend, 0)
+    def open_links():
+        pl.semaphore_wait(barrier, n_dev - 1)
+        for other in far_planes:
+            relay_copy(hi, other).start()
+
+    first_part = packs // group // 2
+    lax.fori_loop(0, first_part, attend, 0)
+    pl.when(me >= 2)(open_links)
+    lax.fori_loop(first_part, packs // group, attend, 0)
+    pl.when(me < 2)(open_links)
 
     mixed = mix_rows[...]
     mean = jnp.sum(mixed * mixed, axis=1, keepdims=True) * (1.0 / v_width)
@@ -330,28 +401,46 @@
     laid = mm(head_out, shifted)
     own = iota(laid.shape, 1) // v_width == lax.rem(iota(laid.shape, 0), per_kv)
     laid = jnp.where(own, laid, 0.0).astype(BF16)
+    picked_rows = lax.dot_general(
+        row_choice, laid, (((0,), (0,)), ((), ())), preferred_element_type=F32
+    )
+    for e in range(n_dev):
+        head_rows[e] = picked_rows[e * capacity : (e + 1) * capacity, :].astype(BF16)
+    head_slots[tp * n_ep + ep] = head_rows[me]
+    for other_ep, other_tp in peers:
+        remote(
+            head_rows.at[other_ep * n_tp + other_tp],
+            head_slots.at[tp * n_ep + ep],
+            slot_sem,
+            other_ep,
+            other_tp,
+        ).start()
     gather = (seqs, seqs * per_kv)
     heads[tp] = mm(hot(iota(gather, 1) // per_kv == iota(gather, 0)), laid).astype(BF16)
 
-    pl.semaphore_wait(barrier, n_dev - 1)
-
-    def head_copy(step):
-        other = lax.rem(tp + step, n_tp)
-        return pltpu.make_async_remote_copy(
-            src_ref=heads.at[tp],
-            dst_ref=heads.at[tp],
-            send_sem=head_send.at[step],
-            recv_sem=head_recv.at[step],
-            device_id=(ep, other),
-            device_id_type=MESH,
+    for t in range(1, n_tp):
+        remote(heads.at[tp], heads.at[tp], head_sem, ep, lax.rem(tp + t, n_tp)).start()
+    relay[hi] = tokens[:, pl.ds(pl.multiple_of(tp * share, share), share)]
+    for index, source in enumerate([hi] + far_planes[::-1]):
+        if index:
+            relay_copy(source, lax.rem(hi + 1, n_hi)).wait_recv()
+        rows_out = lax.dot_general(
+            relay_pick[source], relay[source], (((0,), (0,)), ((), ())), preferred_element_type=F32
         )
-
-    head_copies = [head_copy(step) for step in range(1, n_tp)]
-    for copy in head_copies:
-        copy.start()
+        for q in range(plane):
+            packed[source, q] = rows_out[q * capacity : (q + 1) * capacity, :].astype(BF16)
+        arrived[tp, source, lo] = packed[source, spot_in_plane]
+        for q in range(1, plane):
+            other = lax.rem(spot_in_plane + q, plane)
+            remote(
+                packed.at[source, other],
+                arrived.at[tp, source, lo],
+                disp_sem,
+                hi * n_lo + other // n_tp,
+                lax.rem(other, n_tp),
+            ).start()
     weights[3].wait()
-    for copy in head_copies:
-        copy.wait_recv()
+    whole(heads, heads, head_sem, n_tp - 1).wait_recv()
     depth = heads.shape[2]
     projected = jnp.zeros((seqs, width), F32)
     for i in range(n_tp):
@@ -362,33 +451,6 @@
         resid[i] = residual[:, i * share : (i + 1) * share]
     ffn_in = rms(residual, ffn_gain[...]).astype(BF16)
 
-    sorted_rows = lax.dot_general(
-        dispatch, ffn_in, (((0,), (0,)), ((), ())), preferred_element_type=F32
-    )
-    for e in range(n_ep):
-        packed[e] = sorted_rows[e * capacity : (e + 1) * capacity, :].astype(BF16)
-    arrived[ep] = packed[ep]
-
-    def disp_copy(step):
-        other = lax.rem(ep + step, n_ep)
-        return pltpu.make_async_remote_copy(
-            src_ref=packed.at[other],
-            dst_ref=arrived.at[ep],
-            send_sem=disp_send.at[step],
-            recv_sem=disp_recv.at[step],
-            device_id=(other, tp),
-            device_id_type=MESH,
-        )
-
-    def loop(make, act, count):
-        def body(step, carry):
-            act(make(step))
-            return carry
-
-        lax.fori_loop(1, count, body, 0)
-
-    loop(disp_copy, lambda copy: copy.start(), n_ep)
-
     for i in range(4, 7):
         weights[i].wait()
     shared_act = (jax.nn.silu(mm(ffn_in, sg[...])) * mm(ffn_in, su[...])).astype(BF16)
@@ -396,25 +458,25 @@
     for i in range(n_tp):
         share_out[i] = shared_part[:, i * share : (i + 1) * share].astype(BF16)
 
-    def share_copy(step):
-        other = lax.rem(tp + step, n_tp)
-        return pltpu.make_async_remote_copy(
-            src_ref=share_out.at[other],
-            dst_ref=share_in.at[step],
-            send_sem=share_send.at[step],
-            recv_sem=share_recv.at[step],
-            device_id=(ep, other),
-            device_id_type=MESH,
-        )
-
-    share_copies = [share_copy(step) for step in range(1, n_tp)]
-    for copy in share_copies:
-        copy.start()
-
+    for t in range(1, n_tp):
+        other = lax.rem(tp + t, n_tp)
+        remote(share_out.at[other], share_in.at[t - 1], share_sem, ep, other).start()
+
+    whole(head_rows, head_slots, slot_sem, n_dev - 1).wait_recv()
+    projected = jnp.zeros((n_ep * capacity, width), F32)
+    for i in range(n_tp):
+        piece = flat_slots(head_slots[i * n_ep : (i + 1) * n_ep]).astype(BF16)
+        piece = mm(piece, wo[i * depth : (i + 1) * depth, :])
+        projected = projected + piece.astype(BF16).astype(F32)
+    relayed_all = packed.at[:, pl.ds(0, plane - 1)]
+    remote(relayed_all, relayed_all, disp_sem, ep, lax.rem(tp + 1, n_tp)).wait_recv()
     for i in range(7, 10):
         weights[i].wait()
-    loop(disp_copy, lambda copy: copy.wait_recv(), n_ep)
-    flat = flat_slots(arrived[...]).astype(BF16)
+    rows_in = [
+        flat_slots(arrived[i].reshape(n_ep, capacity, share)) for i in range(n_tp)
+    ]
+    residual = (jnp.concatenate(rows_in, axis=1) + projected).astype(BF16).astype(F32)
+    flat = rms(residual, ffn_gain[...]).astype(BF16)
     act = (jax.nn.silu(mm(flat, eg[...])) * mm(flat, eu[...])).astype(BF16)
     result = mm(act, ed[...])
     for e in range(n_ep):
@@ -424,31 +486,25 @@
             ].astype(BF16)
     returned[me] = computed[me]
 
-    def back_copy(step):
-        other = lax.rem(me + step, n_dev)
-        return pltpu.make_async_remote_copy(
-            src_ref=computed.at[other],
-            dst_ref=returned.at[me],
-            send_sem=back_send.at[step],
-            recv_sem=back_recv.at[step],
-            device_id=(other // n_tp, lax.rem(other, n_tp)),
-            device_id_type=MESH,
-        )
-
-    loop(back_copy, lambda copy: copy.start(), n_dev)
+    for other_ep, other_tp in peers:
+        remote(
+            computed.at[other_ep * n_tp + other_tp], returned.at[me], back_sem, other_ep, other_tp
+        ).start()
     total = resid[tp] + share_out[tp].astype(F32)
-    for step, copy in enumerate(share_copies):
-        copy.wait_recv()
-        total = total + share_in[step + 1].astype(F32)
-    loop(back_copy, lambda copy: copy.wait_recv(), n_dev)
+    whole(share_out, share_in, share_sem, n_tp - 1).wait_recv()
+    for i in range(n_tp - 1):
+        total = total + share_in[i].astype(F32)
+    whole(heads, heads, head_sem, n_tp - 1).wait_send()
+    whole(share_out, share_in, share_sem, n_tp - 1).wait_send()
+    whole(head_rows, head_slots, slot_sem, n_dev - 1).wait_send()
+    whole(relay, relay, relay_sem, n_hi - 1).wait_send()
+    remote(relayed_all, relayed_all, disp_sem, ep, lax.rem(tp + 1, n_tp)).wait_send()
+    whole(computed, returned, back_sem, n_dev - 1).wait_recv()
     back = flat_slots(returned[...]).astype(BF16)
     routed = mm(mix_high, back) + mm(mix_low, back)
     out[...] = (total + routed).astype(BF16)
 
-    for copy in head_copies + share_copies:
-        copy.wait_send()
-    loop(disp_copy, lambda copy: copy.wait_send(), n_ep)
-    loop(back_copy, lambda copy: copy.wait_send(), n_dev)
+    whole(computed, returned, back_sem, n_dev - 1).wait_send()
 
 
 def shards(
@@ -481,6 +537,9 @@
     n_dev = n_ep * n_tp
     capacity = max(2, 2 * seqs * routing.shape[1] // (w_exp_gate.shape[0] * n_dev))
     share = width // n_tp
+    n_lo = 2 if n_ep % 2 == 0 else 1
+    n_hi = n_ep // n_lo
+    plane = n_lo * n_tp
     side = lanes // v_width * 2
     packs = seqs // side
     rows = seqs * per_kv
@@ -527,9 +586,13 @@
             pltpu.VMEM((rows, fold), F32),
             pltpu.VMEM((rows, fold), F32),
             pltpu.VMEM((n_tp, seqs, per_kv * v_width), BF16),
+            pltpu.VMEM((n_dev, capacity, per_kv * v_width), BF16),
+            pltpu.VMEM((n_dev, capacity, per_kv * v_width), BF16),
             pltpu.VMEM((n_tp, seqs, share), F32),
-            pltpu.VMEM((n_ep, capacity, width), BF16),
-            pltpu.VMEM((n_ep, capacity, width), BF16),
+            pltpu.VMEM((n_hi, seqs, plane * capacity), BF16),
+            pltpu.VMEM((n_hi, seqs, share), BF16),
+            pltpu.VMEM((n_hi, plane, capacity, share), BF16),
+            pltpu.VMEM((n_tp, n_hi, n_lo, capacity, share), BF16),
             pltpu.VMEM((n_dev, capacity, share), BF16),
             pltpu.VMEM((n_dev, capacity, share), BF16),
             pltpu.VMEM((n_tp, seqs, share), BF16),
@@ -537,14 +600,12 @@
             dma((len(small),)),
             dma((packs,)),
             dma((10,)),
-            dma((n_tp,)),
-            dma((n_tp,)),
-            dma((n_ep,)),
-            dma((n_ep,)),
-            dma((n_dev,)),
-            dma((n_dev,)),
-            dma((n_tp,)),
-            dma((n_tp,)),
+            dma((2,)),
+            dma((2,)),
+            dma((1 + n_hi,)),
+            dma((2,)),
+            dma((2,)),
+            dma((2,)),
         ],
         compiler_params=pltpu.CompilerParams(
             collective_id=0, has_side_effects=True, vmem_limit_bytes=60 * 1024 * 1024

time: 30 us -> 26.4 us (0.88)
  Pallas kernels: 29.3 us -> 25.7 us
    pallas_call x1, Pallas kernels: 29.3 us -> 25.7 us  [shards(): pl.pallas_call(functools.partial(layer, n_ep, n_tp, capacity, group), out...]
where the time goes in v2:
time: 26.4 us; the launch traced here: 26.3 us
  Pallas kernels  25.7 us (97%)
  local copies, waits for them, and re-layouts  0.62 us (2%)
    pallas_call x1, Pallas kernels, shards(): pl.pallas_call(functools.partial(layer, n_ep, n_tp, capacity, group), out...  25.7 us
    unnamed x1, local copies, waits for them, and re-layouts  0.62 us

profile of v2, /device:TPU:0, one launch (start us, length us, event | category | flops | bytes accessed | tf_op | source)
XLA Modules:
  0.0 26.3 jit_solution(9751687227781486283)
XLA Ops:
  0.0 25.7 %shard_map.181 = bf16[32,512]{1,0:T(8,128)(2,1)S(1)} custom-call(s32[32]{0:T(128)} %lengths_hbm.1, f32[4]{0:T(128)} %lambdas_hbm.1, bf16[32,2048]{1,0:T(8,128)(2,1)} %tokens_hbm.1, f32[1,2048]{1,0:T(1,128)} %bitcast.9, f32[1,64]{1,0:T(1,128)} %bitcast.13, f32[1,2048]{1,0:T(1,128)} %bitcast.10, s32[4,256]{1,0:T(4,128)} %bitcast.11, f32[4,32]{1,0:T(4,128)} %bitcast.12, ...), custom_call_target="tpu_custom_call" | custom-call | tf_op jit(solution)/shard_map/pallas_call | solution.py:577
  25.7 0.6 %copy.21 = bf16[32,512]{1,0:T(8,128)(2,1)} copy(bf16[32,512]{1,0:T(8,128)(2,1)S(1)} %shard_map.181) | data formatting | bytes 65536

commit v3 on v2

--- a/solution.py
+++ b/solution.py
@@ -188,14 +188,11 @@
     for i in range(2, 8):
         inputs[i].start()
 
-    def greet(step, carry):
+    for step in range(1, n_dev):
         other = lax.rem(me + step, n_dev)
         pl.semaphore_signal(
             barrier, inc=1, device_id=(other // n_tp, lax.rem(other, n_tp)), device_id_type=MESH
         )
-        return carry
-
-    lax.fori_loop(1, n_dev, greet, 0)
 
     def start_kv(pack, carry):
         kv_copy(pack).start()
@@ -232,7 +229,15 @@
         for t in range(n_tp)
     ]
     peers += [(ep, lax.rem(tp + t, n_tp)) for t in range(1, n_tp)]
-    far_planes = [far_first(k, hi, n_hi) for k in range(n_hi - 1)]
+    half_planes = n_hi // 2 if n_hi % 2 == 0 else n_hi
+    upper = hi // half_planes
+    near_planes = [
+        upper * half_planes + lax.rem(hi + k, half_planes) for k in range(1, half_planes)
+    ]
+    across = n_hi // half_planes - 1
+    far_planes = [
+        half_planes - upper + k * (1 - 2 * upper) for k in range(across * half_planes)
+    ]
 
     def relay_copy(source, target):
         return pltpu.make_async_remote_copy(
@@ -247,14 +252,22 @@
     for i in range(2):
         inputs[i].wait()
     normed = rms(tokens[...].astype(F32), attn_gain[...]).astype(BF16)
-    top_count, batch = routing.shape
-    picked = (iota((seqs, batch), 0) + ep * seqs == iota((seqs, batch), 1)).astype(F32)
     for i in range(2, 4):
         inputs[i].wait()
-    own_ids = exact(picked, routing[...].astype(F32), 1).astype(jnp.int32)
-    own_weights = exact(
-        (iota((seqs, seqs), 0) == iota((seqs, seqs), 1)).astype(F32), route_weights[...], 1
-    )
+    top_count, batch = routing.shape
+
+    def lookup(select, table):
+        if n_dev > 256:
+            return exact(select, table, 1)
+        return mm_t(select.astype(BF16), table.astype(BF16))
+
+    picked = (iota((seqs, batch), 0) + ep * seqs == iota((seqs, batch), 1)).astype(F32)
+    ids = routing[...].astype(F32)
+    own_ids = lookup(picked, ids).astype(jnp.int32)
+    high = route_weights[...].astype(BF16)
+    low = (route_weights[...] - high.astype(F32)).astype(BF16)
+    same = hot(iota((seqs, seqs), 0) == iota((seqs, seqs), 1))
+    own_weights = mm_t(same, high) + mm_t(same, low)
     before = hot(iota((seqs, seqs), 1) < iota((seqs, seqs), 0))
 
     def slots(count, expert_of):
@@ -276,7 +289,7 @@
     relayed = n_hi * seqs
     row = iota((relayed, batch), 0)
     picked = (row // seqs * n_lo + lo) * seqs + lax.rem(row, seqs) == iota((relayed, batch), 1)
-    relay_ids = exact(picked.astype(F32), routing[...].astype(F32), 1).astype(jnp.int32)
+    relay_ids = lookup(picked.astype(F32), ids).astype(jnp.int32)
     column = iota((relayed, plane * capacity), 1)
     expert = hi * plane + column // capacity
     hit = functools.reduce(
@@ -323,7 +336,7 @@
 
     for i in range(4, 8):
         inputs[i].wait()
-    wide_gain = exact(jnp.broadcast_to(head_gain[...], (8, v_width)), tile.astype(F32), 0)
+    wide_gain = jnp.concatenate([head_gain[...]] * side, axis=1)
     row = iota((block, 1), 0)
     factor = jnp.ones((block, 1), F32)
     for g in range(per_kv):
@@ -384,23 +397,33 @@
 
     def open_links():
         pl.semaphore_wait(barrier, n_dev - 1)
-        for other in far_planes:
+        outer = (hi != half_planes - 1 + upper).astype(jnp.int32)
+        for k in range(len(far_planes)):
+            k = k + outer * (half_planes - 1 - 2 * k)
+            relay_copy(hi, half_planes - upper + k * (1 - 2 * upper)).start()
+        for other in near_planes:
             relay_copy(hi, other).start()
 
     first_part = packs // group // 2
+    pl.when(hi == n_hi - 1)(open_links)
     lax.fori_loop(0, first_part, attend, 0)
-    pl.when(me >= 2)(open_links)
+    pl.when((me >= 2) & (hi < n_hi - 1))(open_links)
     lax.fori_loop(first_part, packs // group, attend, 0)
     pl.when(me < 2)(open_links)
 
     mixed = mix_rows[...]
     mean = jnp.sum(mixed * mixed, axis=1, keepdims=True) * (1.0 / v_width)
-    head_out = (mixed * lax.rsqrt(mean + epsilon) * wide_gain[:1]).astype(BF16)
+    head_out = (mixed * lax.rsqrt(mean + epsilon) * wide_gain).astype(BF16)
     unfold = (fold_width, per_kv * v_width)
     shifted = hot(lax.rem(iota(unfold, 1), v_width) == lax.rem(iota(unfold, 0), v_width))
     laid = mm(head_out, shifted)
     own = iota(laid.shape, 1) // v_width == lax.rem(iota(laid.shape, 0), per_kv)
     laid = jnp.where(own, laid, 0.0).astype(BF16)
+    gather = (seqs, seqs * per_kv)
+    heads[tp] = mm(hot(iota(gather, 1) // per_kv == iota(gather, 0)), laid).astype(BF16)
+
+    for t in range(1, n_tp):
+        remote(heads.at[tp], heads.at[tp], head_sem, ep, lax.rem(tp + t, n_tp)).start()
     picked_rows = lax.dot_general(
         row_choice, laid, (((0,), (0,)), ((), ())), preferred_element_type=F32
     )
@@ -415,13 +438,8 @@
             other_ep,
             other_tp,
         ).start()
-    gather = (seqs, seqs * per_kv)
-    heads[tp] = mm(hot(iota(gather, 1) // per_kv == iota(gather, 0)), laid).astype(BF16)
-
-    for t in range(1, n_tp):
-        remote(heads.at[tp], heads.at[tp], head_sem, ep, lax.rem(tp + t, n_tp)).start()
     relay[hi] = tokens[:, pl.ds(pl.multiple_of(tp * share, share), share)]
-    for index, source in enumerate([hi] + far_planes[::-1]):
+    for index, source in enumerate([hi] + near_planes + far_planes):
         if index:
             relay_copy(source, lax.rem(hi + 1, n_hi)).wait_recv()
         rows_out = lax.dot_general(
@@ -485,7 +503,6 @@
                 e * capacity : (e + 1) * capacity, t * share : (t + 1) * share
             ].astype(BF16)
     returned[me] = computed[me]
-
     for other_ep, other_tp in peers:
         remote(
             computed.at[other_ep * n_tp + other_tp], returned.at[me], back_sem, other_ep, other_tp

time: 26.4 us -> 25.5 us (0.966)
  Pallas kernels: 25.7 us -> 24.8 us
    pallas_call x1, Pallas kernels: 25.7 us -> 24.8 us  [shards(): pl.pallas_call(functools.partial(layer, n_ep, n_tp, capacity, group), out...]
where the time goes in v3:
time: 25.5 us; the launch traced here: 25.4 us
  Pallas kernels  24.8 us (97%)
  local copies, waits for them, and re-layouts  0.62 us (2%)
    pallas_call x1, Pallas kernels, shards(): pl.pallas_call(functools.partial(layer, n_ep, n_tp, capacity, group), out...  24.8 us
    unnamed x1, local copies, waits for them, and re-layouts  0.62 us

profile of v3, /device:TPU:0, one launch (start us, length us, event | category | flops | bytes accessed | tf_op | source)
XLA Modules:
  0.0 25.4 jit_solution(16551130528304360537)
XLA Ops:
  0.0 24.8 %shard_map.181 = bf16[32,512]{1,0:T(8,128)(2,1)S(1)} custom-call(s32[32]{0:T(128)} %lengths_hbm.1, f32[4]{0:T(128)} %lambdas_hbm.1, bf16[32,2048]{1,0:T(8,128)(2,1)} %tokens_hbm.1, f32[1,2048]{1,0:T(1,128)} %bitcast.9, f32[1,64]{1,0:T(1,128)} %bitcast.13, f32[1,2048]{1,0:T(1,128)} %bitcast.10, s32[4,256]{1,0:T(4,128)} %bitcast.11, f32[4,32]{1,0:T(4,128)} %bitcast.12, ...), custom_call_target="tpu_custom_call" | custom-call | tf_op jit(solution)/shard_map/pallas_call | solution.py:594
  24.8 0.6 %copy.21 = bf16[32,512]{1,0:T(8,128)(2,1)} copy(bf16[32,512]{1,0:T(8,128)(2,1)S(1)} %shard_map.181) | data formatting | bytes 65536

commit v4 on v3

--- a/solution.py
+++ b/solution.py
@@ -395,6 +395,23 @@
             mix_rows[spots, :] = jnp.where(own, mixed, 0.0)
         return carry
 
+    def spread_rows(source):
+        rows_out = lax.dot_general(
+            relay_pick[source], relay[source], (((0,), (0,)), ((), ())), preferred_element_type=F32
+        )
+        for q in range(plane):
+            packed[source, q] = rows_out[q * capacity : (q + 1) * capacity, :].astype(BF16)
+        arrived[tp, source, lo] = packed[source, spot_in_plane]
+        for q in range(1, plane):
+            other = lax.rem(spot_in_plane + q, plane)
+            remote(
+                packed.at[source, other],
+                arrived.at[tp, source, lo],
+                disp_sem,
+                hi * n_lo + other // n_tp,
+                lax.rem(other, n_tp),
+            ).start()
+
     def open_links():
         pl.semaphore_wait(barrier, n_dev - 1)
         outer = (hi != half_planes - 1 + upper).astype(jnp.int32)
@@ -403,6 +420,8 @@
             relay_copy(hi, half_planes - upper + k * (1 - 2 * upper)).start()
         for other in near_planes:
             relay_copy(hi, other).start()
+        relay[hi] = tokens[:, pl.ds(pl.multiple_of(tp * share, share), share)]
+        spread_rows(hi)
 
     first_part = packs // group // 2
     pl.when(hi == n_hi - 1)(open_links)
@@ -438,25 +457,9 @@
             other_ep,
             other_tp,
         ).start()
-    relay[hi] = tokens[:, pl.ds(pl.multiple_of(tp * share, share), share)]
-    for index, source in enumerate([hi] + near_planes + far_planes):
-        if index:
-            relay_copy(source, lax.rem(hi + 1, n_hi)).wait_recv()
-        rows_out = lax.dot_general(
-            relay_pick[source], relay[source], (((0,), (0,)), ((), ())), preferred_element_type=F32
-        )
-        for q in range(plane):
-            packed[source, q] = rows_out[q * capacity : (q + 1) * capacity, :].astype(BF16)
-        arrived[tp, source, lo] = packed[source, spot_in_plane]
-        for q in range(1, plane):
-            other = lax.rem(spot_in_plane + q, plane)
-            remote(
-                packed.at[source, other],
-                arrived.at[tp, source, lo],
-                disp_sem,
-                hi * n_lo + other // n_tp,
-                lax.rem(other, n_tp),
-            ).start()
+    for source in near_planes + far_planes:
+        relay_copy(source, lax.rem(hi + 1, n_hi)).wait_recv()
+        spread_rows(source)
     weights[3].wait()
     whole(heads, heads, head_sem, n_tp - 1).wait_recv()
     depth = heads.shape[2]
@@ -503,7 +506,9 @@
                 e * capacity : (e + 1) * capacity, t * share : (t + 1) * share
             ].astype(BF16)
     returned[me] = computed[me]
-    for other_ep, other_tp in peers:
+    rising = [k + (k >= ep).astype(jnp.int32) for k in range(n_ep - 1)]
+    rising = [(other, lax.rem(tp + t, n_tp)) for other in rising for t in range(n_tp)]
+    for other_ep, other_tp in rising + peers[len(rising) :]:
         remote(
             computed.at[other_ep * n_tp + other_tp], returned.at[me], back_sem, other_ep, other_tp
         ).start()

time: 25.5 us -> 24.9 us (0.976)
  Pallas kernels: 24.8 us -> 24.1 us
    pallas_call x1, Pallas kernels: 24.8 us -> 24.1 us  [shards(): pl.pallas_call(functools.partial(layer, n_ep, n_tp, capacity, group), out...]
where the time goes in v4:
time: 24.9 us; the launch traced here: 24.8 us
  Pallas kernels  24.1 us (97%)
  local copies, waits for them, and re-layouts  0.62 us (2%)
    pallas_call x1, Pallas kernels, shards(): pl.pallas_call(functools.partial(layer, n_ep, n_tp, capacity, group), out...  24.1 us
    unnamed x1, local copies, waits for them, and re-layouts  0.62 us

profile of v4, /device:TPU:0, one launch (start us, length us, event | category | flops | bytes accessed | tf_op | source)
XLA Modules:
  0.0 24.8 jit_solution(236794047959857480)
XLA Ops:
  0.0 24.1 %shard_map.181 = bf16[32,512]{1,0:T(8,128)(2,1)S(1)} custom-call(s32[32]{0:T(128)} %lengths_hbm.1, f32[4]{0:T(128)} %lambdas_hbm.1, bf16[32,2048]{1,0:T(8,128)(2,1)} %tokens_hbm.1, f32[1,2048]{1,0:T(1,128)} %bitcast.9, f32[1,64]{1,0:T(1,128)} %bitcast.13, f32[1,2048]{1,0:T(1,128)} %bitcast.10, s32[4,256]{1,0:T(4,128)} %bitcast.11, f32[4,32]{1,0:T(4,128)} %bitcast.12, ...), custom_call_target="tpu_custom_call" | custom-call | tf_op jit(solution)/shard_map/pallas_call | solution.py:599
  24.2 0.6 %copy.21 = bf16[32,512]{1,0:T(8,128)(2,1)} copy(bf16[32,512]{1,0:T(8,128)(2,1)S(1)} %shard_map.181) | data formatting | bytes 65536
